TPU v7x, 32 devices: a whole 2x2x4 slice. The times are simulated.
32 devices in a mesh: kv: 8 (over z, y), tp: 4 (over x, core).
Axes of the slice: x: 2, y: 2, z: 4, core: 2. Of those that a mesh axis runs over, the one named last changes fastest.
Arguments:
- queries: bfloat16 [1024, 1024], P('kv', 'tp'), may hold values from -6 to 6
- keys: bfloat16 [1024, 512], P('kv', 'tp'), may hold values from -6 to 6
- values: bfloat16 [1024, 512], P('kv', 'tp'), may hold values from -6 to 6
- hidden: bfloat16 [1024, 2048], P('kv'), may hold values from -6 to 6
- log_sums: float32 [2, 1024, 16], P(None, 'kv', 'tp'), may hold values from -1 to 12
- gates: float32 [2, 1024, 16], P(None, 'kv', 'tp'), may hold values from 0.1 to 0.9
- branch_out: bfloat16 [2, 1024, 1024], P(None, 'kv', 'tp'), may hold values from -6 to 6
- cotangent: bfloat16 [1024, 1024], P('kv', 'tp'), may hold values from -6 to 6
- chosen: int32 [8, 8, 48], P(None, 'tp'), may hold values from -1 to 31, as said below
Outputs:
- grad_queries: float32 [1024, 1024], P('kv', 'tp')
- grad_keys: float32 [1024, 512], P('kv', 'tp')
- grad_values: float32 [1024, 512], P('kv', 'tp')
- grad_weight: float32 [2048, 1024], P('kv', 'tp')
Inputs may be any that keep to these rules, and one draw needn't show every extreme that they name: `chosen`: each list holds global block numbers or -1. All live entries of one list name blocks of distinct owners, owner = entry // 4, none later than the list's range; list d holds min(48, d + 1) live entries, and they come first.
All inputs are finite; a program needn't handle non-finite values.
Results may differ from a plain program's by a relative error of at most 0.0055.
Values may be sent and summed in bfloat16 or wider, within the bound.
A program may use at most 64 MiB of HBM per device.

v0:
```python
import jax
import jax.numpy as jnp
from jax import lax
from jax.sharding import PartitionSpec as P

DH = 64
BLK = 32
TOPN = 12
SUB = 4
CMP = 32


def branch_grads(query_rows, key_rows, value_rows, seen, log_rows, delta_rows, cot_rows, scale):
    wide = jnp.float32
    scores = jnp.einsum("tgre,gme->grtm", query_rows, key_rows, preferred_element_type=wide) * scale
    log_here = jnp.transpose(log_rows, (1, 2, 0))[..., None]
    delta_here = jnp.transpose(delta_rows, (1, 2, 0))[..., None]
    probs = jnp.where(seen[:, None], jnp.exp(scores - log_here), 0.0)
    probs_low = probs.astype(jnp.bfloat16)
    value_grad = jnp.einsum("grtm,tgre->gme", probs_low, cot_rows, preferred_element_type=wide)
    prob_grad = jnp.einsum("tgre,gme->grtm", cot_rows, value_rows, preferred_element_type=wide)
    score_low = (probs * (prob_grad - delta_here)).astype(jnp.bfloat16)
    query_grad = (
        jnp.einsum("grtm,gme->tgre", score_low, key_rows, preferred_element_type=wide) * scale
    )
    key_grad = (
        jnp.einsum("grtm,tgre->gme", score_low, query_rows, preferred_element_type=wide) * scale
    )
    return (query_grad, key_grad, value_grad)


def shards(queries, keys, values, hidden, log_sums, gates, branch_out, cotangent, chosen):
    wide = jnp.float32
    rows_here = queries.shape[0]
    heads = queries.shape[1] // DH
    groups = keys.shape[1] // DH
    group_heads = heads // groups
    per_block = rows_here // BLK
    per_summary = rows_here // CMP
    blocks_all = chosen.shape[0]
    nsel = chosen.shape[2]
    qrows = rows_here // SUB
    scale = DH ** (-0.5)
    grads_each = jax.vmap(branch_grads, in_axes=(0, 0, 0, 0, 0, 0, 0, None))
    place = lax.axis_index("kv")
    position = place * rows_here + jnp.arange(rows_here, dtype=jnp.int32)
    gated = gates[..., None] * cotangent.reshape(rows_here, heads, DH).astype(wide)[None]
    delta_all = jnp.sum(gated * branch_out.reshape(2, rows_here, heads, DH).astype(wide), -1)
    delta_all = delta_all.reshape(2, rows_here, groups, group_heads)
    gated_low = gated.astype(jnp.bfloat16).reshape(2, rows_here, groups, group_heads, DH)
    log_all = log_sums.reshape(2, rows_here, groups, group_heads)
    query_all = queries.reshape(rows_here, groups, group_heads, DH)
    pairs = jnp.concatenate(
        [keys.reshape(rows_here, groups, DH), values.reshape(rows_here, groups, DH)], -1
    )
    means = jnp.mean(pairs.reshape(per_summary, CMP, groups, 2 * DH).astype(wide), 1).astype(
        jnp.bfloat16
    )
    summaries = lax.all_gather(means, "kv", axis=0, tiled=True)
    summary_count = summaries.shape[0]
    sum_keys = jnp.transpose(summaries[..., :DH], (1, 0, 2))
    sum_values = jnp.transpose(summaries[..., DH:], (1, 0, 2))
    summary_end = jnp.arange(summary_count, dtype=jnp.int32) * CMP + CMP - 1
    summary_seen = (summary_end[None, :] <= position[:, None])[None]
    query_sum, key_sum, value_sum = branch_grads(
        query_all, sum_keys, sum_values, summary_seen, log_all[0], delta_all[0], gated_low[0], scale
    )
    summary_term = jnp.transpose(jnp.concatenate([key_sum, value_sum], -1), (1, 0, 2))
    listing = lax.dynamic_index_in_dim(chosen, place, 0, keepdims=False)
    live = listing >= 0
    safe = jnp.maximum(listing, 0)
    owner = safe // per_block
    group_index = jnp.arange(groups, dtype=jnp.int32)
    hits = (chosen >= 0) & (chosen // per_block == place)
    wanted = jnp.sum(jnp.where(hits, chosen % per_block, 0), -1)
    asked = jnp.any(hits, -1)
    row_target = safe[..., None] * BLK + jnp.arange(BLK, dtype=jnp.int32)
    pair_blocks = pairs.reshape(per_block, BLK, groups, 2 * DH)
    outbound = pair_blocks[wanted, :, group_index[None, :], :]
    arrived = lax.all_to_all(outbound, "kv", split_axis=0, concat_axis=0, tiled=True)
    picked = arrived[owner, group_index[:, None]]

    def by_sub(array):
        rest = array.shape[3:]
        moved = array.reshape((groups, SUB, TOPN * BLK) + rest)
        return jnp.swapaxes(moved, 0, 1)

    picked_sub = by_sub(picked)
    picked_keys = picked_sub[..., :DH]
    picked_values = picked_sub[..., DH:]
    live_rows = by_sub(jnp.broadcast_to(live[..., None], (groups, nsel, BLK)))
    key_position = by_sub(row_target)
    sub_position = position.reshape(SUB, qrows)
    block_seen = live_rows[:, :, None, :] & (
        key_position[:, :, None, :] <= sub_position[:, None, :, None]
    )
    query_sel, key_sel, value_sel = grads_each(
        query_all.reshape(SUB, qrows, groups, group_heads, DH),
        picked_keys,
        picked_values,
        block_seen,
        log_all[1].reshape(SUB, qrows, groups, group_heads),
        delta_all[1].reshape(SUB, qrows, groups, group_heads),
        gated_low[1].reshape(SUB, qrows, groups, group_heads, DH),
        scale,
    )
    query_sel = query_sel.reshape(rows_here, groups, group_heads, DH)
    key_sel = jnp.swapaxes(key_sel, 0, 1).reshape(groups, nsel, BLK, DH)
    value_sel = jnp.swapaxes(value_sel, 0, 1).reshape(groups, nsel, BLK, DH)
    slot_grads = jnp.concatenate([key_sel, value_sel], -1)
    slot_grads = slot_grads * live[..., None, None].astype(wide)
    outgoing = (
        jnp.zeros((blocks_all, groups, BLK, 2 * DH), wide)
        .at[owner, group_index[:, None]]
        .add(slot_grads)
    )
    summary_out = jnp.transpose(
        summary_term.reshape(blocks_all, per_summary, groups, 2 * DH), (0, 2, 1, 3)
    )
    both_out = jnp.concatenate([outgoing, summary_out], 2)
    both_in = lax.all_to_all(
        both_out.astype(jnp.bfloat16), "kv", split_axis=0, concat_axis=0, tiled=True
    ).astype(both_out.dtype)
    incoming = both_in[:, :, :BLK]
    summary_mine = jnp.transpose(jnp.sum(both_in[:, :, BLK:], 0), (1, 0, 2))
    selector = (
        (wanted[..., None] == jnp.arange(per_block, dtype=jnp.int32)) & asked[..., None]
    ).astype(wide)
    block_sums = jnp.einsum("rgb,rgkc->bkgc", selector, incoming, precision=lax.Precision.HIGHEST)
    pair_grads = (
        block_sums.reshape(rows_here, groups, 2 * DH) + jnp.repeat(summary_mine, CMP, axis=0) / CMP
    )
    grad_queries = (query_sum + query_sel).reshape(rows_here, heads * DH)
    query_low = grad_queries.astype(jnp.bfloat16)
    grad_weight = lax.psum_scatter(
        lax.dot_general(
            hidden, query_low, (((0,), (0,)), ((), ())), preferred_element_type=jnp.float32
        ),
        "kv",
        scatter_dimension=0,
        tiled=True,
    )
    grad_keys = pair_grads[..., :DH].reshape(rows_here, groups * DH)
    grad_values = pair_grads[..., DH:].reshape(rows_here, groups * DH)
    return (grad_queries, grad_keys, grad_values, grad_weight)


def solution(mesh):
    return jax.shard_map(
        shards,
        mesh=mesh,
        in_specs=(
            P("kv", "tp"),
            P("kv", "tp"),
            P("kv", "tp"),
            P("kv", None),
            P(None, "kv", "tp"),
            P(None, "kv", "tp"),
            P(None, "kv", "tp"),
            P("kv", "tp"),
            P(None, "tp", None),
        ),
        out_specs=(P("kv", "tp"), P("kv", "tp"), P("kv", "tp"), P("kv", "tp")),
        check_vma=False,
    )
```

profile of v0, /device:TPU:0, one launch (start us, length us, event | category | flops | bytes accessed | tf_op | source)
XLA Modules:
  0.0 136.0 jit_solution(15902463175480948571)
XLA Ops:
  7.2 1.0 fusion.44
  8.2 0.9 fusion.33
  9.1 0.1 copy.157
  9.2 0.1 copy.158
  9.3 0.1 reshape.249
  9.4 0.8 concatenate.26
  10.3 0.8 concatenate.27
  11.1 0.1 convert_reduce_fusion
  11.3 1.3 gather_fusion
  12.5 7.3 %all-to-all-start = ((bf16[8,2,32,128]{3,2,1,0:T(8,128)(2,1)}), bf16[8,2,32,128]{3,2,1,0:T(8,128)(2,1)S(1)}, u32[]{:S(2)}, u32[]{:S(2)}) async-start(bf16[8,2,32,128]{3,2,1,0:T(8,128)(2,1)} %bitcast.20), calls=%async_computation | async-start | bytes 262144 | tf_op jit(solution)/shard_map/all_to_all | solution.py:80
  19.9 0.7 multiply_bitcast_fusion.1
  20.6 0.7 fusion.45
  21.3 0.7 or_select_fusion
  22.0 1.0 copy.153
  22.9 1.0 reshape_reshape.3
  23.9 0.1 reshape.255
  24.0 0.1 add.117
  24.1 0.1 broadcast_in_dim.36
  24.2 0.1 reshape.239
  24.4 0.1 add.115
  24.5 26.6 %all_gather.3 = bf16[32,2,128]{2,1,0:T(2,128)(2,1)S(1)} all-gather(bf16[4,2,128]{2,1,0:T(2,128)(2,1)S(1)} %multiply_convert_fusion.1), channel_id=1, replica_groups=mesh['kv'=8,'tp'=4] {'kv'}, dimensions={0}, use_global_device_ids=true | all-gather | bytes 18432 | tf_op jit(solution)/shard_map/all_gather | solution.py:59
  51.1 0.1 fusion.48
  51.2 0.1 copy.155
  51.4 0.1 copy.156
  51.7 0.1 compare_and_fusion
  51.8 0.1 fusion.18
  52.0 0.1 reshape_squeeze.9
  52.1 0.1 reshape_squeeze.11
  52.2 0.1 copy.164
  52.3 0.1 fusion.19
  52.4 1.2 gather_fusion.1
  53.6 0.4 copy.159
  54.0 0.3 fusion.5
  54.3 0.3 fusion.8
  54.6 0.3 fusion.9
  54.9 0.3 copy-done.1
  55.2 0.1 copy.168
  55.3 0.2 fusion.12
  55.5 1.8 %convolution_bitcast_fusion = f32[2048,256]{0,1:T(8,128)} fusion(bf16[128,2048]{1,0:T(8,128)(2,1)S(1)} %copy-done, f32[128,256]{0,1:T(8,128)S(1)} %bitcast.188), kind=kOutput, calls=%fused_computation.3 | convolution fusion | flops 134250496 | bytes 2752512 | tf_op jit(solution)/shard_map/dot_general | solution.py:136
  57.3 0.1 reshape.261
  57.4 0.1 fusion.21
  57.5 0.1 fusion.22
  57.7 0.1 pad_maximum_fusion.2
  57.8 0.4 copy-done.3
  58.2 0.3 fusion.7
  58.5 0.5 copy.170
  59.0 1.4 %convolution_bitcast_fusion.1 = f32[2,4,384,64]{2,3,0,1:T(8,128)S(1)} fusion(f32[4,2,2,32,384]{4,3,2,1,0:T(8,128)} %copy-done.1, bf16[4,32,2,2,64]{4,1,0,3,2:T(8,128)(2,1)S(1)} %bitcast.187), kind=kOutput, calls=%fused_computation.5 | convolution fusion | flops 25362432 | bytes 1638400 | tf_op jit(solution)/shard_map/vmap(grtm,tgre->gme)/dot_general | solution.py:20
  60.4 1.6 %copy.172 = f32[2,4,384,64]{3,2,1,0:T(8,128)} copy(f32[2,4,384,64]{2,3,0,1:T(8,128)S(1)} %convolution_bitcast_fusion.1) | data formatting | bytes 1572864 | tf_op jit(solution)/shard_map/transpose | solution.py:109
  62.1 3.2 %maximum_multiply_fusion = f32[2,48,32,128]{3,2,1,0:T(8,128)} fusion(f32[2,48,32,64]{3,2,1,0:T(8,128)} %bitcast.180, f32[2,48,32,64]{3,2,1,0:T(8,128)S(1)} %bitcast.178, f32[2,48]{1,0:T(2,128)S(1)} %get-tuple-element.30), kind=kLoop, calls=%fused_computation.4 | loop fusion | flops 786432 | bytes 3146112 | tf_op jit(solution)/shard_map/mul | solution.py:111
  65.3 9.7 %scatter_fusion = f32[8,2,32,128]{3,2,1,0:T(8,128)S(1)} fusion(f32[8,2,32,128]{3,2,1,0:T(8,128)S(1)} %broadcast_in_dim.39, s32[96]{0:T(128)S(1)} %reshape.261, f32[96,32,128]{2,1,0:T(8,128)} %bitcast.179), kind=kCustom, calls=%fused_computation.2 | custom fusion | flops 393216 | bytes 4719360 | tf_op jit(solution)/shard_map/scatter-add | solution.py:115
  75.1 0.8 copy.174
  75.9 3.9 %all-to-all-start.1 = ((bf16[8,2,36,128]{3,1,2,0:T(2,128)(2,1)}), bf16[8,2,36,128]{3,1,2,0:T(2,128)(2,1)S(1)}, u32[]{:S(2)}, u32[]{:S(2)}) async-start(bf16[8,2,36,128]{3,1,2,0:T(2,128)(2,1)} %copy.174), calls=%async_computation.1 | async-start | bytes 294912 | tf_op jit(solution)/shard_map/all_to_all | solution.py:121
  79.8 0.1 copy.177
  79.9 0.8 copy.182
  80.6 8.5 %all-to-all-done.1 = bf16[8,2,36,128]{3,1,2,0:T(2,128)(2,1)S(1)} async-done(((bf16[8,2,36,128]{3,1,2,0:T(2,128)(2,1)}), bf16[8,2,36,128]{3,1,2,0:T(2,128)(2,1)S(1)}, u32[]{:S(2)}, u32[]{:S(2)}) %all-to-all-start.1) | async-done | bytes 147488 | tf_op jit(solution)/shard_map/all_to_all | solution.py:121
  89.2 0.1 slice.80
  89.3 0.3 fusion.10
  89.6 0.1 fusion.46
  89.7 0.1 copy.181
  89.8 0.7 copy.184
  90.5 0.1 copy.180
  90.6 0.7 copy.183
  91.3 36.1 %reduce-scatter.2.cloned.1.call-done = f32[256,256]{0,1:T(8,128)} async-done(((f32[2048,256]{0,1:T(8,128)}), f32[256,256]{0,1:T(8,128)}) %reduce-scatter.2.cloned.1.call-update) | async-done | bytes 262160 | tf_op jit(solution)/shard_map/reduce_scatter | solution.py:135
  127.4 1.8 %copy.185 = f32[256,256]{1,0:T(8,128)} copy(f32[256,256]{0,1:T(8,128)} %reduce-scatter.2.cloned.1.call-done) | data formatting | bytes 524288
  (47 shorter events, 0.6 us)
Async XLA Ops:
  7.2 48.4 %copy-start = (bf16[128,2048]{1,0:T(8,128)(2,1)S(1)}, bf16[128,2048]{1,0:T(8,128)(2,1)}, u32[]{:S(2)}) copy-start(bf16[128,2048]{1,0:T(8,128)(2,1)} %param.12) | copy-start | bytes 1572868
  7.2 16.8 %copy-start.7 = (f32[2,128,4]{1,2,0:T(4,128)S(1)}, f32[2,128,4]{1,2,0:T(4,128)}, u32[]{:S(2)}) copy-start(f32[2,128,4]{1,2,0:T(4,128)} %param.13) | copy-start | bytes 12292
  7.2 44.0 %copy-start.5 = (bf16[128,256]{1,0:T(8,128)(2,1)S(1)}, bf16[128,256]{1,0:T(8,128)(2,1)}, u32[]{:S(2)}) copy-start(bf16[128,256]{1,0:T(8,128)(2,1)} %param.16) | copy-start | bytes 196612
  7.2 44.2 %copy-start.4 = (bf16[2,128,256]{2,1,0:T(8,128)(2,1)S(1)}, bf16[2,128,256]{2,1,0:T(8,128)(2,1)}, u32[]{:S(2)}) copy-start(bf16[2,128,256]{2,1,0:T(8,128)(2,1)} %param.15) | copy-start | bytes 393220
  7.2 44.3 %copy-start.6 = (f32[2,128,4]{1,2,0:T(4,128)S(1)}, f32[2,128,4]{1,2,0:T(4,128)}, u32[]{:S(2)}) copy-start(f32[2,128,4]{1,2,0:T(4,128)} %param.14) | copy-start | bytes 12292
  12.5 39.9 %all-to-all-start = ((bf16[8,2,32,128]{3,2,1,0:T(8,128)(2,1)}), bf16[8,2,32,128]{3,2,1,0:T(8,128)(2,1)S(1)}, u32[]{:S(2)}, u32[]{:S(2)}) async-start(bf16[8,2,32,128]{3,2,1,0:T(8,128)(2,1)} %bitcast.20), calls=%async_computation | async-start | bytes 262144 | tf_op jit(solution)/shard_map/all_to_all | solution.py:80
  19.8 107.6 %reduce-scatter.2.cloned.1.call-start = ((), (), s32[]{:S(2)}) async-start(), calls=%async_computation.3 | async-start | bytes 2359296 | tf_op jit(solution)/shard_map/reduce_scatter | solution.py:135
  23.9 30.1 %copy-start.2 = (bf16[4,32,2,2,64]{4,3,2,1,0:T(2,128)(2,1)}, bf16[4,32,2,2,64]{4,3,2,1,0:T(2,128)(2,1)S(1)}, u32[]{:S(2)}) copy-start(bf16[4,32,2,2,64]{4,3,2,1,0:T(2,128)(2,1)S(1)} %reshape_reshape.3) | copy-start | bytes 196612
  54.3 0.9 copy-start.1
  57.3 0.9 copy-start.3
  75.9 13.3 %all-to-all-start.1 = ((bf16[8,2,36,128]{3,1,2,0:T(2,128)(2,1)}), bf16[8,2,36,128]{3,1,2,0:T(2,128)(2,1)S(1)}, u32[]{:S(2)}, u32[]{:S(2)}) async-start(bf16[8,2,36,128]{3,1,2,0:T(2,128)(2,1)} %copy.174), calls=%async_computation.1 | async-start | bytes 294912 | tf_op jit(solution)/shard_map/all_to_all | solution.py:121
Sparse Core Ops, SparseCore 0:
  57.4 69.8 reduce-scatter.1
where the time goes:
time: 137 us; the launch traced here: 136 us
  waiting for transfers between devices  44.6 us (33%)
  blocking collectives  26.6 us (19%)
  other arithmetic  17.5 us (13%)
  local copies, waits for them, and re-layouts  16.2 us (12%)
  between operations  14.5 us (11%)
  starting transfers between devices  11.3 us (8%)
  matrix products  5.35 us (4%)
    reduce_scatter x1, waiting for transfers between devices, shards(): lax.psum_scatter(lax.dot_general(hidden, query_low, (((0,), (0,)), ((), (...  36.1 us
    all_gather x1, blocking collectives, shards(): summaries = lax.all_gather(means, 'kv', axis=0, tiled=True)  26.6 us
    scatter-add x1, other arithmetic, shards(): outgoing = jnp.zeros((blocks_all, groups, BLK, 2 * DH), wide).at[owner, g...  9.74 us
    all_to_all x1, waiting for transfers between devices, shards(): lax.all_to_all(both_out.astype(jnp.bfloat16), 'kv', split_axis=0, concat_...  8.53 us
    all_to_all x1, starting transfers between devices, shards(): lax.all_to_all(outbound, 'kv', split_axis=0, concat_axis=0, tiled=True)  7.31 us
    unnamed x23, local copies, waits for them, and re-layouts  5.95 us
    all_to_all x1, starting transfers between devices, shards(): lax.all_to_all(both_out.astype(jnp.bfloat16), 'kv', split_axis=0, concat_...  3.92 us
    mul x1, other arithmetic, shards(): slot_grads = slot_grads * live[..., None, None].astype(wide)  3.19 us
  transfers between devices with their start and end apart: 3, of which 2 were waited for; matrix products, arithmetic and copies ran while one was open for 20% of the time, Pallas kernels for 0%

commit v1 on v0

--- a/solution.py
+++ b/solution.py
@@ -1,3 +1,4 @@
+import functools
 import jax
 import jax.numpy as jnp
 from jax import lax
@@ -8,6 +9,21 @@
 TOPN = 12
 SUB = 4
 CMP = 32
+
+
+def _advance_ranges(xin, mesh_dim):
+    return jnp.concatenate(
+        lax.all_to_all(
+            jnp.stack([xin for _ in range(lax.psum(1, mesh_dim))]),
+            mesh_dim,
+            split_axis=0,
+            concat_axis=0,
+        ),
+        0,
+    )
+
+
+types_bind = functools.partial(_advance_ranges, mesh_dim="kv")
 
 
 def branch_grads(query_rows, key_rows, value_rows, seen, log_rows, delta_rows, cot_rows, scale):
@@ -56,7 +72,7 @@
     means = jnp.mean(pairs.reshape(per_summary, CMP, groups, 2 * DH).astype(wide), 1).astype(
         jnp.bfloat16
     )
-    summaries = lax.all_gather(means, "kv", axis=0, tiled=True)
+    summaries = types_bind(means)
     summary_count = summaries.shape[0]
     sum_keys = jnp.transpose(summaries[..., :DH], (1, 0, 2))
     sum_values = jnp.transpose(summaries[..., DH:], (1, 0, 2))

time: 137 us -> 123 us (0.90)
  blocking collectives: 26.6 us -> 0 us
  waiting for transfers between devices: 44.6 us -> 50.2 us
  starting transfers between devices: 11.3 us -> 16.7 us
    all_gather x1 -> x0, blocking collectives: 26.6 us -> none  [shards(): summaries = lax.all_gather(means, 'kv', axis=0, tiled=True)]
    all_to_all x0 -> x1, starting transfers between devices: none -> 7.31 us  [_advance_ranges(): lax.all_to_all(jnp.stack([xin for _ in range(lax.psum(1, mesh_dim))]), me...]
    all_to_all x1, waiting for transfers between devices: 0.01 us -> 6.93 us  [shards(): lax.all_to_all(outbound, 'kv', split_axis=0, concat_axis=0, tiled=True)]
    unnamed x23 -> x19, local copies, waits for them, and re-layouts: 5.95 us -> 6.85 us
  transfers between devices with their start and end apart: 3 -> 4, of which waited for: 2 -> 3; matrix products, arithmetic and copies ran while one was open for 20% -> 25% of each run, Pallas kernels for 0% -> 0%
where the time goes in v1:
time: 123 us; the launch traced here: 122 us
  waiting for transfers between devices  50.2 us (41%)
  local copies, waits for them, and re-layouts  17.5 us (14%)
  other arithmetic  17.5 us (14%)
  starting transfers between devices  16.7 us (14%)
  between operations  14.5 us (12%)
  matrix products  5.42 us (4%)
    reduce_scatter x1, waiting for transfers between devices, shards(): lax.psum_scatter(lax.dot_general(hidden, query_low, (((0,), (0,)), ((), (...  35.4 us
    scatter-add x1, other arithmetic, shards(): outgoing = jnp.zeros((blocks_all, groups, BLK, 2 * DH), wide).at[owner, g...  9.74 us
    all_to_all x1, waiting for transfers between devices, shards(): lax.all_to_all(both_out.astype(jnp.bfloat16), 'kv', split_axis=0, concat_...  7.89 us
    all_to_all x1, starting transfers between devices, _advance_ranges(): lax.all_to_all(jnp.stack([xin for _ in range(lax.psum(1, mesh_dim))]), me...  7.31 us
    all_to_all x1, waiting for transfers between devices, shards(): lax.all_to_all(outbound, 'kv', split_axis=0, concat_axis=0, tiled=True)  6.93 us
    unnamed x19, local copies, waits for them, and re-layouts  6.85 us
    all_to_all x1, starting transfers between devices, shards(): lax.all_to_all(outbound, 'kv', split_axis=0, concat_axis=0, tiled=True)  5.99 us
    all_to_all x1, starting transfers between devices, shards(): lax.all_to_all(both_out.astype(jnp.bfloat16), 'kv', split_axis=0, concat_...  3.38 us
  transfers between devices with their start and end apart: 4, of which 3 were waited for; matrix products, arithmetic and copies ran while one was open for 25% of the time, Pallas kernels for 0%

profile of v1, /device:TPU:0, one launch (start us, length us, event | category | flops | bytes accessed | tf_op | source)
XLA Modules:
  0.0 121.8 jit_solution(283484282575222371)
XLA Ops:
  7.2 0.9 concatenate.26
  8.1 0.8 concatenate.27
  9.0 0.1 convert_reduce_fusion
  9.1 0.6 stack.2
  9.7 7.3 %all-to-all-start = ((bf16[8,4,2,128]{3,1,2,0:T(4,128)(2,1)}), bf16[8,4,2,128]{3,1,2,0:T(4,128)(2,1)S(1)}, u32[]{:S(2)}, u32[]{:S(2)}) async-start(bf16[8,4,2,128]{3,1,2,0:T(4,128)(2,1)} %stack.2), calls=%async_computation | async-start | bytes 32768 | tf_op jit(solution)/shard_map/all_to_all | solution.py:16
  17.1 0.7 multiply_bitcast_fusion.1
  17.8 0.7 fusion.46
  18.4 0.7 or_select_fusion
  19.1 0.9 fusion.45
  20.1 0.7 fusion.50
  20.8 0.9 fusion.33
  21.7 0.1 copy.193
  21.8 0.1 add.117
  22.0 0.1 reshape.245
  22.1 0.1 add.115
  22.3 1.0 copy.191
  23.2 1.0 copy.192
  24.5 0.1 compare_and_fusion
  24.6 0.1 copy.190
  24.7 0.1 reshape_reshape.3
  24.9 0.1 reshape.261
  25.0 0.1 copy.194
  25.0 0.1 reshape.255
  25.1 0.1 reshape_squeeze.9
  25.2 0.1 reshape_squeeze.11
  25.3 0.1 copy.200
  25.4 1.3 %gather_fusion = bf16[16,32,128]{2,1,0:T(8,128)(2,1)} fusion(bf16[4,32,2,128]{3,1,2,0:T(8,128)(2,1)S(1)} %get-tuple-element.39, s32[16]{0:T(128)S(1)} %reshape.255), kind=kCustom, calls=%fused_computation | custom fusion | bytes 262272 | tf_op jit(solution)/shard_map/gather | solution.py:95
  26.7 6.0 %all-to-all-start.1 = ((bf16[8,2,32,128]{3,2,1,0:T(8,128)(2,1)}), bf16[8,2,32,128]{3,2,1,0:T(8,128)(2,1)S(1)}, u32[]{:S(2)}, u32[]{:S(2)}) async-start(bf16[8,2,32,128]{3,2,1,0:T(8,128)(2,1)} %bitcast.21), calls=%async_computation.1 | async-start | bytes 262144 | tf_op jit(solution)/shard_map/all_to_all | solution.py:96
  32.8 0.1 fusion.18
  32.9 0.2 fusion.19
  33.1 6.9 %all-to-all-done.1 = bf16[8,2,32,128]{3,2,1,0:T(8,128)(2,1)S(1)} async-done(((bf16[8,2,32,128]{3,2,1,0:T(8,128)(2,1)}), bf16[8,2,32,128]{3,2,1,0:T(8,128)(2,1)S(1)}, u32[]{:S(2)}, u32[]{:S(2)}) %all-to-all-start.1) | async-done | bytes 131104 | tf_op jit(solution)/shard_map/all_to_all | solution.py:96
  40.0 1.2 gather_fusion.1
  41.2 0.4 copy.195
  41.6 0.3 fusion.5
  41.9 0.3 fusion.8
  42.2 0.3 fusion.9
  42.5 0.3 copy-done.1
  42.8 0.1 copy.204
  42.9 0.2 fusion.12
  43.1 1.8 %convolution_bitcast_fusion = f32[2048,256]{0,1:T(8,128)} fusion(bf16[128,2048]{1,0:T(8,128)(2,1)S(1)} %copy-done, f32[128,256]{0,1:T(8,128)S(1)} %bitcast.189), kind=kOutput, calls=%fused_computation.3 | convolution fusion | flops 134250496 | bytes 2752512 | tf_op jit(solution)/shard_map/dot_general | solution.py:152
  44.9 0.1 reshape.267
  45.0 0.1 fusion.21
  45.1 0.1 fusion.22
  45.3 0.1 pad_maximum_fusion.2
  45.4 0.4 copy-done.3
  45.8 0.3 fusion.7
  46.1 0.5 copy.206
  46.6 1.4 %convolution_bitcast_fusion.1 = f32[2,4,384,64]{2,3,0,1:T(8,128)S(1)} fusion(f32[4,2,2,32,384]{4,3,2,1,0:T(8,128)} %copy-done.1, bf16[4,32,2,2,64]{4,1,0,3,2:T(8,128)(2,1)S(1)} %bitcast.188), kind=kOutput, calls=%fused_computation.5 | convolution fusion | flops 25362432 | bytes 1638400 | tf_op jit(solution)/shard_map/vmap(grtm,tgre->gme)/dot_general | solution.py:36
  48.0 1.6 %copy.208 = f32[2,4,384,64]{3,2,1,0:T(8,128)} copy(f32[2,4,384,64]{2,3,0,1:T(8,128)S(1)} %convolution_bitcast_fusion.1) | data formatting | bytes 1572864 | tf_op jit(solution)/shard_map/transpose | solution.py:125
  49.7 3.2 %maximum_multiply_fusion = f32[2,48,32,128]{3,2,1,0:T(8,128)} fusion(f32[2,48,32,64]{3,2,1,0:T(8,128)} %bitcast.181, f32[2,48,32,64]{3,2,1,0:T(8,128)S(1)} %bitcast.179, f32[2,48]{1,0:T(2,128)S(1)} %get-tuple-element.34), kind=kLoop, calls=%fused_computation.4 | loop fusion | flops 786432 | bytes 3146112 | tf_op jit(solution)/shard_map/mul | solution.py:127
  52.9 9.7 %scatter_fusion = f32[8,2,32,128]{3,2,1,0:T(8,128)S(1)} fusion(f32[8,2,32,128]{3,2,1,0:T(8,128)S(1)} %broadcast_in_dim.39, s32[96]{0:T(128)S(1)} %reshape.267, f32[96,32,128]{2,1,0:T(8,128)} %bitcast.180), kind=kCustom, calls=%fused_computation.2 | custom fusion | flops 393216 | bytes 4719360 | tf_op jit(solution)/shard_map/scatter-add | solution.py:131
  62.7 0.8 copy.210
  63.5 3.4 %all-to-all-start.2 = ((bf16[8,2,36,128]{3,1,2,0:T(2,128)(2,1)}), bf16[8,2,36,128]{3,1,2,0:T(2,128)(2,1)S(1)}, u32[]{:S(2)}, u32[]{:S(2)}) async-start(bf16[8,2,36,128]{3,1,2,0:T(2,128)(2,1)} %copy.210), calls=%async_computation.2 | async-start | bytes 294912 | tf_op jit(solution)/shard_map/all_to_all | solution.py:137
  66.9 0.1 copy.213
  67.0 0.8 copy.218
  67.7 7.9 %all-to-all-done.2 = bf16[8,2,36,128]{3,1,2,0:T(2,128)(2,1)S(1)} async-done(((bf16[8,2,36,128]{3,1,2,0:T(2,128)(2,1)}), bf16[8,2,36,128]{3,1,2,0:T(2,128)(2,1)S(1)}, u32[]{:S(2)}, u32[]{:S(2)}) %all-to-all-start.2) | async-done | bytes 147488 | tf_op jit(solution)/shard_map/all_to_all | solution.py:137
  75.7 0.1 slice.80
  75.8 0.3 fusion.10
  76.0 0.1 fusion.47
  76.1 0.1 copy.217
  76.2 0.7 copy.220
  77.0 0.7 copy.219
  77.8 35.4 %reduce-scatter.2.cloned.1.call-done = f32[256,256]{0,1:T(8,128)} async-done(((f32[2048,256]{0,1:T(8,128)}), f32[256,256]{0,1:T(8,128)}) %reduce-scatter.2.cloned.1.call-update) | async-done | bytes 262160 | tf_op jit(solution)/shard_map/reduce_scatter | solution.py:151
  113.2 1.8 %copy.221 = f32[256,256]{1,0:T(8,128)} copy(f32[256,256]{0,1:T(8,128)} %reduce-scatter.2.cloned.1.call-done) | data formatting | bytes 524288
  (45 shorter events, 0.7 us)
Async XLA Ops:
  7.2 36.0 %copy-start = (bf16[128,2048]{1,0:T(8,128)(2,1)S(1)}, bf16[128,2048]{1,0:T(8,128)(2,1)}, u32[]{:S(2)}) copy-start(bf16[128,2048]{1,0:T(8,128)(2,1)} %param.12) | copy-start | bytes 1572868
  7.2 17.1 %copy-start.5 = (f32[2,128,4]{1,2,0:T(4,128)S(1)}, f32[2,128,4]{1,2,0:T(4,128)}, u32[]{:S(2)}) copy-start(f32[2,128,4]{1,2,0:T(4,128)} %param.14) | copy-start | bytes 12292
  7.2 17.4 %copy-start.4 = (bf16[128,256]{1,0:T(8,128)(2,1)S(1)}, bf16[128,256]{1,0:T(8,128)(2,1)}, u32[]{:S(2)}) copy-start(bf16[128,256]{1,0:T(8,128)(2,1)} %param.9) | copy-start | bytes 196612
  9.7 17.0 %all-to-all-start = ((bf16[8,4,2,128]{3,1,2,0:T(4,128)(2,1)}), bf16[8,4,2,128]{3,1,2,0:T(4,128)(2,1)S(1)}, u32[]{:S(2)}, u32[]{:S(2)}) async-start(bf16[8,4,2,128]{3,1,2,0:T(4,128)(2,1)} %stack.2), calls=%async_computation | async-start | bytes 32768 | tf_op jit(solution)/shard_map/all_to_all | solution.py:16
  24.9 16.7 %copy-start.2 = (bf16[4,32,2,2,64]{4,3,2,1,0:T(2,128)(2,1)}, bf16[4,32,2,2,64]{4,3,2,1,0:T(2,128)(2,1)S(1)}, u32[]{:S(2)}) copy-start(bf16[4,32,2,2,64]{4,3,2,1,0:T(2,128)(2,1)S(1)} %reshape_reshape.3) | copy-start | bytes 196612
  26.7 13.3 %all-to-all-start.1 = ((bf16[8,2,32,128]{3,2,1,0:T(8,128)(2,1)}), bf16[8,2,32,128]{3,2,1,0:T(8,128)(2,1)S(1)}, u32[]{:S(2)}, u32[]{:S(2)}) async-start(bf16[8,2,32,128]{3,2,1,0:T(8,128)(2,1)} %bitcast.21), calls=%async_computation.1 | async-start | bytes 262144 | tf_op jit(solution)/shard_map/all_to_all | solution.py:96
  32.7 80.5 %reduce-scatter.2.cloned.1.call-start = ((), (), s32[]{:S(2)}) async-start(), calls=%async_computation.4 | async-start | bytes 2359296 | tf_op jit(solution)/shard_map/reduce_scatter | solution.py:151
  41.9 0.9 copy-start.1
  44.9 0.9 copy-start.3
  63.5 12.1 %all-to-all-start.2 = ((bf16[8,2,36,128]{3,1,2,0:T(2,128)(2,1)}), bf16[8,2,36,128]{3,1,2,0:T(2,128)(2,1)S(1)}, u32[]{:S(2)}, u32[]{:S(2)}) async-start(bf16[8,2,36,128]{3,1,2,0:T(2,128)(2,1)} %copy.210), calls=%async_computation.2 | async-start | bytes 294912 | tf_op jit(solution)/shard_map/all_to_all | solution.py:137
Sparse Core Ops, SparseCore 0:
  45.0 68.0 reduce-scatter.1
